TPU v7x, 32 devices: a whole 2x2x4 slice. The times are simulated.
32 devices in a mesh: rep: 2 (over x), fs: 4 (over z), tp: 4 (over y, core).
Axes of the slice: x: 2, y: 2, z: 4, core: 2. Of those that a mesh axis runs over, the one named last changes fastest.
Arguments:
- tokens: bfloat16 [4096, 2048], P(('rep', 'fs', 'tp')), may hold values from -6 to 6
- norm_gain: float32 [2048], replicated, may hold values from 0.1 to 1.9
- gate_weight: float32 [2048, 5632], P('fs', 'tp'), may hold values from -0.125 to 0.125
- gate_scale: float32 [5632], P('tp'), may hold values from 0.5 to 2
- up_weight: float32 [2048, 5632], P('fs', 'tp'), may hold values from -0.125 to 0.125
- up_scale: float32 [5632], P('tp'), may hold values from 0.5 to 2
- down_weight: float32 [5632, 2048], P('tp', 'fs'), may hold values from -0.078125 to 0.078125
- down_scale: float32 [2048], P('fs'), may hold values from 0.5 to 2
Outputs:
- mixed: bfloat16 [4096, 2048], P(('rep', 'fs', 'tp'))
All inputs are finite; a program needn't handle non-finite values.
Results may differ from a plain program's by a relative error of at most 0.014.
Values may be sent and summed in bfloat16 or wider, within the bound.
A program may use at most 64 MiB of HBM per device.

v0:
```python
import jax
import jax.numpy as jnp
from jax import lax
from jax.sharding import PartitionSpec as P


def shards(
    tokens, norm_gain, gate_weight, gate_scale, up_weight, up_scale, down_weight, down_scale
):
    n_rep = lax.axis_size("rep")
    rep = lax.axis_index("rep")
    width = gate_weight.shape[1] // n_rep
    start = rep * width

    def part(array, axis):
        return lax.dynamic_slice_in_dim(array, start, width, axis)

    flat = tokens.astype(jnp.float32)
    mean_square = jnp.mean(flat * flat, axis=-1, keepdims=True)
    inverse = lax.rsqrt(mean_square + 1e-06)
    normed = (flat * inverse * norm_gain).astype(jnp.bfloat16)
    group = lax.all_gather(normed, ("rep", "tp"), axis=0, tiled=True)
    gate_low = part(gate_weight, 1).astype(jnp.bfloat16)
    up_low = part(up_weight, 1).astype(jnp.bfloat16)
    down_low = part(down_weight, 0).astype(jnp.bfloat16)
    gate = jnp.dot(
        group,
        lax.all_gather(gate_low, "fs", axis=0, tiled=True),
        preferred_element_type=jnp.float32,
    )
    up = jnp.dot(
        group, lax.all_gather(up_low, "fs", axis=0, tiled=True), preferred_element_type=jnp.float32
    )
    down_full = lax.all_gather(down_low, "fs", axis=1, tiled=True)
    gate = gate * part(gate_scale, 0)
    up = up * part(up_scale, 0)
    hidden = (jax.nn.silu(gate) * up).astype(jnp.bfloat16)
    scales = lax.all_gather(down_scale, "fs", axis=0, tiled=True)
    total = lax.psum_scatter(
        jnp.dot(hidden, down_full, preferred_element_type=jnp.float32).astype(jnp.bfloat16),
        ("rep", "tp"),
        scatter_dimension=0,
        tiled=True,
    ).astype(jnp.float32)
    return (total * scales).astype(jnp.bfloat16)


def solution(mesh):
    in_specs = (
        P(("rep", "fs", "tp"), None),
        P(),
        P("fs", "tp"),
        P("tp"),
        P("fs", "tp"),
        P("tp"),
        P("tp", "fs"),
        P("fs"),
    )
    out_specs = P(("rep", "fs", "tp"), None)
    return jax.shard_map(shards, mesh=mesh, in_specs=in_specs, out_specs=out_specs, check_vma=False)
```

profile of v0, /device:TPU:0, one launch (start us, length us, event | category | flops | bytes accessed | tf_op | source)
XLA Modules:
  0.0 308.1 jit_solution(6207909742359432319)
XLA Ops:
  6.5 0.0 copy-start
  6.5 0.0 copy-start.1
  6.5 0.0 copy-start.2
  6.5 0.0 all-gather.8.cloned.1.call-start
  6.6 1.8 copy-done
  8.4 1.2 dynamic-slice_convert_fusion.1
  9.6 0.0 all-gather.8.cloned.1.call-update
  9.6 0.0 all-gather.6.cloned.1.call-start
  9.7 1.2 fusion
  10.9 0.0 copy-done.1
  10.9 0.0 copy-done.2
  10.9 0.0 copy-start.4
  10.9 0.0 copy-start.5
  10.9 1.0 fusion.2
  11.9 0.0 all-gather.6.cloned.1.call-update
  11.9 0.0 all-gather.10.cloned.1.call-start
  12.0 2.7 dynamic-slice_convert_fusion
  14.7 0.0 all-gather.10.cloned.1.call-update
  14.8 0.0 all-gather.12.cloned.1.call-start
  14.8 2.3 dynamic-slice_convert_fusion.2
  17.1 0.0 all-gather.12.cloned.1.call-update
  17.2 0.0 reduce-scatter.2.cloned.1.call-start
  17.2 0.0 copy-done.4
  17.2 0.1 dynamic_slice.16
  17.3 0.0 copy-done.5
  17.3 0.1 dynamic_slice.18
  17.4 58.6 %all-gather.8.cloned.1.call-done = bf16[2048,704]{1,0:T(8,128)(2,1)} async-done(((bf16[512,704]{1,0:T(8,128)(2,1)}), bf16[2048,704]{1,0:T(8,128)(2,1)}) %all-gather.8.cloned.1.call-update) | async-done | bytes 2883600 | tf_op jit(solution)/shard_map/all_gather | solution.py:28
  75.9 37.1 %all-gather.6.cloned.1.call-done = bf16[1024,2048]{1,0:T(8,128)(2,1)} async-done(((bf16[128,2048]{1,0:T(8,128)(2,1)}), bf16[1024,2048]{1,0:T(8,128)(2,1)}) %all-gather.6.cloned.1.call-update) | async-done | bytes 4194320 | tf_op jit(solution)/shard_map/all_gather | solution.py:22
  113.1 7.9 %fusion.4 = f32[1024,704]{0,1:T(8,128)} fusion(bf16[1024,2048]{1,0:T(8,128)(2,1)} %all-gather.6.cloned.1.call-done, bf16[2048,704]{1,0:T(8,128)(2,1)} %all-gather.8.cloned.1.call-done), kind=kOutput, calls=%fused_computation.13 | convolution fusion | flops 2952790016 | bytes 9961472 | tf_op jit(solution)/shard_map/dot_general | solution.py:26
  121.0 57.1 %all-gather.10.cloned.1.call-done = bf16[2048,704]{1,0:T(8,128)(2,1)} async-done(((bf16[512,704]{1,0:T(8,128)(2,1)}), bf16[2048,704]{1,0:T(8,128)(2,1)}) %all-gather.10.cloned.1.call-update) | async-done | bytes 2883600 | tf_op jit(solution)/shard_map/all_gather | solution.py:32
  178.1 59.2 %all-gather.12.cloned.1.call-done = bf16[704,2048]{1,0:T(8,128)(2,1)} async-done(((bf16[704,512]{1,0:T(8,128)(2,1)}), bf16[704,2048]{1,0:T(8,128)(2,1)}) %all-gather.12.cloned.1.call-update) | async-done | bytes 2883600 | tf_op jit(solution)/shard_map/all_gather | solution.py:34
  237.3 12.3 %convolution_convert_fusion = bf16[1024,2048]{1,0:T(8,128)(2,1)} fusion(bf16[704,2048]{1,0:T(8,128)(2,1)} %all-gather.12.cloned.1.call-done, f32[1024,704]{0,1:T(8,128)} %fusion.4, bf16[1024,2048]{1,0:T(8,128)(2,1)} %all-gather.6.cloned.1.call-done, bf16[2048,704]{1,0:T(8,128)(2,1)} %all-gather.10.cloned.1.call-done, f32[704]{0:T(1024)S(1)} %dynamic_slice.18, ...), kind=kOutput, calls=%fused_computation | convolution fusion | flops 5913444352 | bytes 17044992 | tf_op jit(solution)/shard_map/dot_general | solution.py:40
  249.7 0.0 copy-start.3
  249.7 0.0 reduce-scatter.2.cloned.1.call-update
  249.7 0.7 copy-done.3
  250.3 11.9 %all-gather = f32[4,1,512]{2,1,0:T(1,128)S(1)} all-gather(f32[1,1,512]{2,1,0:T(1,128)S(1)} %bitcast.8), channel_id=1, replica_groups=mesh['rep'=2,'fs'=4,'tp'=4] {'fs'}, dimensions={0}, use_global_device_ids=true | all-gather | bytes 10240 | tf_op jit(solution)/shard_map/all_gather | solution.py:38
  262.3 37.4 %reduce-scatter.2.cloned.1.call-done = bf16[128,2048]{1,0:T(8,128)(2,1)} async-done(((bf16[1024,2048]{1,0:T(8,128)(2,1)}), bf16[128,2048]{1,0:T(8,128)(2,1)}) %reduce-scatter.2.cloned.1.call-update) | async-done | bytes 524304 | tf_op jit(solution)/shard_map/reduce_scatter | solution.py:39
  299.7 1.9 multiply_convert_fusion.1
  (1 shorter events, 0.0 us)
Async XLA Ops:
  6.5 1.8 copy-start
  6.5 4.4 %copy-start.1 = (bf16[128,2048]{1,0:T(8,128)(2,1)S(1)}, bf16[128,2048]{1,0:T(8,128)(2,1)}, u32[]{:S(2)}) copy-start(bf16[128,2048]{1,0:T(8,128)(2,1)} %param.8) | copy-start | bytes 1572868
  6.5 4.4 %copy-start.2 = (f32[2048]{0:T(1024)S(1)}, f32[2048]{0:T(1024)}, u32[]{:S(2)}) copy-start(f32[2048]{0:T(1024)} %param.9) | copy-start | bytes 24580
  6.5 69.4 %all-gather.8.cloned.1.call-start = ((), (), s32[]{:S(2)}) async-start(), calls=%async_computation.2 | async-start | bytes 3932160 | tf_op jit(solution)/shard_map/all_gather | solution.py:28
  9.6 103.5 %all-gather.6.cloned.1.call-start = ((), (), s32[]{:S(2)}) async-start(), calls=%async_computation.1 | async-start | bytes 4718592 | tf_op jit(solution)/shard_map/all_gather | solution.py:22
  10.9 6.3 %copy-start.4 = (f32[1408]{0:T(1024)S(1)}, f32[1408]{0:T(1024)}, u32[]{:S(2)}) copy-start(f32[1408]{0:T(1024)} %param.11) | copy-start | bytes 16900
  10.9 6.4 %copy-start.5 = (f32[1408]{0:T(1024)S(1)}, f32[1408]{0:T(1024)}, u32[]{:S(2)}) copy-start(f32[1408]{0:T(1024)} %param.13) | copy-start | bytes 16900
  11.9 166.2 %all-gather.10.cloned.1.call-start = ((), (), s32[]{:S(2)}) async-start(), calls=%async_computation.3 | async-start | bytes 3932160 | tf_op jit(solution)/shard_map/all_gather | solution.py:32
  14.8 222.6 %all-gather.12.cloned.1.call-start = ((), (), s32[]{:S(2)}) async-start(), calls=%async_computation.4 | async-start | bytes 3604480 | tf_op jit(solution)/shard_map/all_gather | solution.py:34
  17.2 282.5 %reduce-scatter.2.cloned.1.call-start = ((), (), s32[]{:S(2)}) async-start(), calls=%async_computation.5 | async-start | bytes 4718592 | tf_op jit(solution)/shard_map/reduce_scatter | solution.py:39
  249.7 0.7 copy-start.3
Sparse Core Ops, SparseCore 0:
  9.7 66.1 all-gather.7
  77.8 35.2 all-gather.5
  114.7 63.4 all-gather.9
  179.6 57.7 all-gather.11
  249.8 49.8 reduce-scatter.1
where the time goes:
time: 308 us
  waiting for transfers between devices  250 us (81%)
  matrix products  20.2 us (7%)
  between operations  13.2 us (4%)
  blocking collectives  11.9 us (4%)
  local copies, waits for them, and re-layouts  8.92 us (3%)
  other arithmetic  4.16 us (1%)
    all_gather x1, waiting for transfers between devices, shards(): down_full = lax.all_gather(down_low, 'fs', axis=1, tiled=True)  59.2 us
    all_gather x1, waiting for transfers between devices, shards(): lax.all_gather(gate_low, 'fs', axis=0, tiled=True)  58.6 us
    all_gather x1, waiting for transfers between devices, shards(): lax.all_gather(up_low, 'fs', axis=0, tiled=True)  57.1 us
    reduce_scatter x1, waiting for transfers between devices, shards(): lax.psum_scatter(jnp.dot(hidden, down_full, preferred_element_type=jnp.fl...  37.4 us
    all_gather x1, waiting for transfers between devices, shards(): group = lax.all_gather(normed, ('rep', 'tp'), axis=0, tiled=True)  37.1 us
    dot_general x1, matrix products, shards(): jnp.dot(hidden, down_full, preferred_element_type=jnp.float32)  12.3 us
    all_gather x1, blocking collectives, shards(): scales = lax.all_gather(down_scale, 'fs', axis=0, tiled=True)  11.9 us
    dot_general x1, matrix products, shards(): jnp.dot(group, lax.all_gather(gate_low, 'fs', axis=0, tiled=True), prefer...  7.9 us
  transfers between devices with their start and end apart: 5, of which 5 were waited for; matrix products, arithmetic and copies ran while one was open for 5% of the time, Pallas kernels for 0%

commit v1 on v0

--- a/solution.py
+++ b/solution.py
@@ -31,7 +31,12 @@
     up = jnp.dot(
         group, lax.all_gather(up_low, "fs", axis=0, tiled=True), preferred_element_type=jnp.float32
     )
-    down_full = lax.all_gather(down_low, "fs", axis=1, tiled=True)
+    ring = [down_low]
+    for hop in range(3):
+        ring.append(lax.ppermute(ring[-1], "fs", [(dev, (dev + 1) % 4) for dev in range(4)]))
+    down_full = jnp.roll(
+        jnp.concatenate(ring[::-1], axis=1), (lax.axis_index("fs") + 1) * ring[0].shape[1], axis=1
+    )
     gate = gate * part(gate_scale, 0)
     up = up * part(up_scale, 0)
     hidden = (jax.nn.silu(gate) * up).astype(jnp.bfloat16)

time: 308 us -> 278 us (0.903)
  waiting for transfers between devices: 250 us -> 187 us
  starting transfers between devices: 0.17 us -> 17.7 us
  local copies, waits for them, and re-layouts: 8.92 us -> 22.5 us
    ppermute x0 -> x3, waiting for transfers between devices: none -> 86.1 us  [shards(): lax.ppermute(ring[-1], 'fs', [(dev, (dev + 1) % 4) for dev in range(4)])]
    all_gather x1 -> x0, waiting for transfers between devices: 59.2 us -> none  [shards(): down_full = lax.all_gather(down_low, 'fs', axis=1, tiled=True)]
    all_gather x1, waiting for transfers between devices: 58.6 us -> 0.01 us  [shards(): lax.all_gather(gate_low, 'fs', axis=0, tiled=True)]
    all_gather x1, waiting for transfers between devices: 37.1 us -> 6.15 us  [shards(): group = lax.all_gather(normed, ('rep', 'tp'), axis=0, tiled=True)]
    ppermute x0 -> x3, starting transfers between devices: none -> 17.6 us  [shards(): lax.ppermute(ring[-1], 'fs', [(dev, (dev + 1) % 4) for dev in range(4)])]
    unnamed x12 -> x21, local copies, waits for them, and re-layouts: 2.48 us -> 15.9 us
  transfers between devices with their start and end apart: 5 -> 7, of which waited for: 5 -> 6; matrix products, arithmetic and copies ran while one was open for 5% -> 10% of each run, Pallas kernels for 0% -> 0%
where the time goes in v1:
time: 278 us
  waiting for transfers between devices  187 us (67%)
  local copies, waits for them, and re-layouts  22.5 us (8%)
  matrix products  20.2 us (7%)
  starting transfers between devices  17.7 us (6%)
  between operations  13.2 us (5%)
  blocking collectives  11.9 us (4%)
  other arithmetic  5.2 us (2%)
    ppermute x3, waiting for transfers between devices, shards(): lax.ppermute(ring[-1], 'fs', [(dev, (dev + 1) % 4) for dev in range(4)])  86.1 us
    all_gather x1, waiting for transfers between devices, shards(): lax.all_gather(up_low, 'fs', axis=0, tiled=True)  57.1 us
    reduce_scatter x1, waiting for transfers between devices, shards(): lax.psum_scatter(jnp.dot(hidden, down_full, preferred_element_type=jnp.fl...  37.4 us
    ppermute x3, starting transfers between devices, shards(): lax.ppermute(ring[-1], 'fs', [(dev, (dev + 1) % 4) for dev in range(4)])  17.6 us
    unnamed x21, local copies, waits for them, and re-layouts  15.9 us
    dot_general x1, matrix products, shards(): jnp.dot(hidden, down_full, preferred_element_type=jnp.float32)  12.3 us
    all_gather x1, blocking collectives, shards(): scales = lax.all_gather(down_scale, 'fs', axis=0, tiled=True)  11.9 us
    dot_general x1, matrix products, shards(): jnp.dot(group, lax.all_gather(gate_low, 'fs', axis=0, tiled=True), prefer...  7.9 us
  transfers between devices with their start and end apart: 7, of which 6 were waited for; matrix products, arithmetic and copies ran while one was open for 10% of the time, Pallas kernels for 0%

profile of v1, /device:TPU:0, one launch (start us, length us, event | category | flops | bytes accessed | tf_op | source)
XLA Modules:
  0.0 277.6 jit_solution(2320724168191950796)
XLA Ops:
  6.5 0.0 copy-start
  6.5 0.0 copy-start.5
  6.5 0.0 copy-start.6
  6.5 0.0 all-gather.7.cloned.1.call-start
  6.6 1.8 copy-done
  8.4 1.2 dynamic-slice_convert_fusion.1
  9.6 0.0 all-gather.7.cloned.1.call-update
  9.6 0.0 all-gather.5.cloned.1.call-start
  9.6 1.2 fusion.1
  10.9 2.0 fusion.3
  12.9 0.0 all-gather.5.cloned.1.call-update
  12.9 0.0 all-gather.9.cloned.1.call-start
  13.0 2.7 dynamic-slice_convert_fusion
  15.7 0.0 all-gather.9.cloned.1.call-update
  15.7 0.0 reduce-scatter.2.cloned.1.call-start
  15.8 1.5 dynamic-slice_convert_fusion.2
  17.3 3.1 %collective-permute-start = (bf16[704,512]{1,0:T(8,128)(2,1)S(1)}, bf16[704,512]{1,0:T(8,128)(2,1)S(1)}, u32[]{:S(2)}, u32[]{:S(2)}) collective-permute-start(bf16[704,512]{1,0:T(8,128)(2,1)S(1)} %dynamic-slice_convert_fusion.2), channel_id=1, source_target_pairs={{0,4},{4,8},{8,12},{12,0},{1,5},{5,9},{9,13},{13,1},{2,6},{6,10},{... | collective-permute-start | bytes 2162696 | tf_op jit(solution)/shard_map/ppermute | solution.py:36
  20.4 32.6 %collective-permute-done = bf16[704,512]{1,0:T(8,128)(2,1)S(1)} collective-permute-done((bf16[704,512]{1,0:T(8,128)(2,1)S(1)}, bf16[704,512]{1,0:T(8,128)(2,1)S(1)}, u32[]{:S(2)}, u32[]{:S(2)}) %collective-permute-start) | collective-permute-done | bytes 720928 | tf_op jit(solution)/shard_map/ppermute | solution.py:36
  52.9 0.0 copy-start.1
  52.9 0.9 copy-done.1
  53.8 14.5 %collective-permute-start.1 = (bf16[704,512]{1,0:T(8,128)(2,1)S(1)}, bf16[704,512]{1,0:T(8,128)(2,1)}, u32[]{:S(2)}, u32[]{:S(2)}) collective-permute-start(bf16[704,512]{1,0:T(8,128)(2,1)S(1)} %collective-permute-done), channel_id=1, source_target_pairs={{0,4},{4,8},{8,12},{12,0},{1,5},{5,9},{9,13},{13,1},{2,6},{6,10},{... | collective-permute-start | bytes 2162696 | tf_op jit(solution)/shard_map/ppermute | solution.py:36
  68.4 35.3 %collective-permute-done.1 = bf16[704,512]{1,0:T(8,128)(2,1)} collective-permute-done((bf16[704,512]{1,0:T(8,128)(2,1)S(1)}, bf16[704,512]{1,0:T(8,128)(2,1)}, u32[]{:S(2)}, u32[]{:S(2)}) %collective-permute-start.1) | collective-permute-done | bytes 720928 | tf_op jit(solution)/shard_map/ppermute | solution.py:36
  103.7 0.0 collective-permute-start.2
  103.7 0.0 copy-done.5
  103.7 0.1 dynamic_slice.20
  103.8 0.0 copy-done.6
  103.8 0.1 dynamic_slice.22
  103.8 0.0 copy-start.3
  103.8 0.0 copy-start.2
  103.8 18.2 %collective-permute-done.2 = bf16[704,512]{1,0:T(8,128)(2,1)} collective-permute-done((bf16[704,512]{1,0:T(8,128)(2,1)}, bf16[704,512]{1,0:T(8,128)(2,1)}, u32[]{:S(2)}, u32[]{:S(2)}) %collective-permute-start.2) | collective-permute-done | bytes 720928 | tf_op jit(solution)/shard_map/ppermute | solution.py:36
  122.1 2.1 constant_dynamic-update-slice_fusion.7
  124.1 2.1 constant_dynamic-update-slice_fusion.6
  126.2 2.3 constant_dynamic-update-slice_fusion.5
  128.5 0.0 copy-done.3
  128.5 1.0 constant_dynamic-update-slice_fusion.4
  129.5 2.1 constant_dynamic-update-slice_fusion.3
  131.6 2.1 constant_dynamic-update-slice_fusion.2
  133.7 0.0 copy-done.2
  133.7 1.0 constant_dynamic-update-slice_fusion.1
  134.6 1.0 constant_dynamic-update-slice_fusion
  135.6 0.0 all-gather.7.cloned.1.call-done
  135.6 6.1 %all-gather.5.cloned.1.call-done = bf16[1024,2048]{1,0:T(8,128)(2,1)} async-done(((bf16[128,2048]{1,0:T(8,128)(2,1)}), bf16[1024,2048]{1,0:T(8,128)(2,1)}) %all-gather.5.cloned.1.call-update) | async-done | bytes 4194320 | tf_op jit(solution)/shard_map/all_gather | solution.py:22
  141.8 7.9 %fusion.6 = f32[1024,704]{0,1:T(8,128)} fusion(bf16[1024,2048]{1,0:T(8,128)(2,1)} %all-gather.5.cloned.1.call-done, bf16[2048,704]{1,0:T(8,128)(2,1)} %all-gather.7.cloned.1.call-done), kind=kOutput, calls=%fused_computation.23 | convolution fusion | flops 2952790016 | bytes 9961472 | tf_op jit(solution)/shard_map/dot_general | solution.py:26
  149.7 57.1 %all-gather.9.cloned.1.call-done = bf16[2048,704]{1,0:T(8,128)(2,1)} async-done(((bf16[512,704]{1,0:T(8,128)(2,1)}), bf16[2048,704]{1,0:T(8,128)(2,1)}) %all-gather.9.cloned.1.call-update) | async-done | bytes 2883600 | tf_op jit(solution)/shard_map/all_gather | solution.py:32
  206.8 12.3 %convolution_convert_fusion = bf16[1024,2048]{1,0:T(8,128)(2,1)} fusion(bf16[704,4096]{1,0:T(8,128)(2,1)} %constant_dynamic-update-slice_fusion, s32[]{:T(128)S(6)} %select_n.22, f32[1024,704]{0,1:T(8,128)} %fusion.6, bf16[1024,2048]{1,0:T(8,128)(2,1)} %all-gather.5.cloned.1.call-done, bf16[2048,704]{1,0:T(8,128)(2,1)} %all-gather.9.cloned.1.call-done, ...), kind=kOutput, calls=%fused_computation | convolution fusion | flops 5913444352 | bytes 17307140 | tf_op jit(solution)/shard_map/dot_general | solution.py:45
  219.1 0.0 copy-start.4
  219.1 0.0 reduce-scatter.2.cloned.1.call-update
  219.1 0.7 copy-done.4
  219.8 11.9 %all-gather = f32[4,1,512]{2,1,0:T(1,128)S(1)} all-gather(f32[1,1,512]{2,1,0:T(1,128)S(1)} %bitcast.7), channel_id=1, replica_groups=mesh['rep'=2,'fs'=4,'tp'=4] {'fs'}, dimensions={0}, use_global_device_ids=true | all-gather | bytes 10240 | tf_op jit(solution)/shard_map/all_gather | solution.py:43
  231.7 37.4 %reduce-scatter.2.cloned.1.call-done = bf16[128,2048]{1,0:T(8,128)(2,1)} async-done(((bf16[1024,2048]{1,0:T(8,128)(2,1)}), bf16[128,2048]{1,0:T(8,128)(2,1)}) %reduce-scatter.2.cloned.1.call-update) | async-done | bytes 524304 | tf_op jit(solution)/shard_map/reduce_scatter | solution.py:44
  269.1 1.9 multiply_convert_fusion.1
  (1 shorter events, 0.0 us)
Async XLA Ops:
  6.5 1.8 copy-start
  6.5 97.1 %copy-start.5 = (f32[1408]{0:T(1024)S(1)}, f32[1408]{0:T(1024)}, u32[]{:S(2)}) copy-start(f32[1408]{0:T(1024)} %param.11) | copy-start | bytes 16900
  6.5 97.2 %copy-start.6 = (f32[1408]{0:T(1024)S(1)}, f32[1408]{0:T(1024)}, u32[]{:S(2)}) copy-start(f32[1408]{0:T(1024)} %param.13) | copy-start | bytes 16900
  6.5 129.1 %all-gather.7.cloned.1.call-start = ((), (), s32[]{:S(2)}) async-start(), calls=%async_computation.2 | async-start | bytes 3932160 | tf_op jit(solution)/shard_map/all_gather | solution.py:28
  9.6 132.2 %all-gather.5.cloned.1.call-start = ((), (), s32[]{:S(2)}) async-start(), calls=%async_computation.1 | async-start | bytes 4718592 | tf_op jit(solution)/shard_map/all_gather | solution.py:22
  12.9 193.9 %all-gather.9.cloned.1.call-start = ((), (), s32[]{:S(2)}) async-start(), calls=%async_computation.3 | async-start | bytes 3932160 | tf_op jit(solution)/shard_map/all_gather | solution.py:32
  15.7 253.4 %reduce-scatter.2.cloned.1.call-start = ((), (), s32[]{:S(2)}) async-start(), calls=%async_computation.4 | async-start | bytes 4718592 | tf_op jit(solution)/shard_map/reduce_scatter | solution.py:44
  17.3 35.7 %collective-permute-start = (bf16[704,512]{1,0:T(8,128)(2,1)S(1)}, bf16[704,512]{1,0:T(8,128)(2,1)S(1)}, u32[]{:S(2)}, u32[]{:S(2)}) collective-permute-start(bf16[704,512]{1,0:T(8,128)(2,1)S(1)} %dynamic-slice_convert_fusion.2), channel_id=1, source_target_pairs={{0,4},{4,8},{8,12},{12,0},{1,5},{5,9},{9,13},{13,1},{2,6},{6,10},{... | collective-permute-start | bytes 2162696 | tf_op jit(solution)/shard_map/ppermute | solution.py:36
  52.9 0.9 copy-start.1
  53.8 49.8 %collective-permute-start.1 = (bf16[704,512]{1,0:T(8,128)(2,1)S(1)}, bf16[704,512]{1,0:T(8,128)(2,1)}, u32[]{:S(2)}, u32[]{:S(2)}) collective-permute-start(bf16[704,512]{1,0:T(8,128)(2,1)S(1)} %collective-permute-done), channel_id=1, source_target_pairs={{0,4},{4,8},{8,12},{12,0},{1,5},{5,9},{9,13},{13,1},{2,6},{6,10},{... | collective-permute-start | bytes 2162696 | tf_op jit(solution)/shard_map/ppermute | solution.py:36
  103.7 18.4 %collective-permute-start.2 = (bf16[704,512]{1,0:T(8,128)(2,1)}, bf16[704,512]{1,0:T(8,128)(2,1)}, u32[]{:S(2)}, u32[]{:S(2)}) collective-permute-start(bf16[704,512]{1,0:T(8,128)(2,1)} %collective-permute-done.1), channel_id=1, source_target_pairs={{0,4},{4,8},{8,12},{12,0},{1,5},{5,9},{9,13},{13,1},{2,6},{6,10},{... | collective-permute-start | bytes 2162696 | tf_op jit(solution)/shard_map/ppermute | solution.py:36
  103.8 24.6 %copy-start.3 = (f32[1408,512]{1,0:T(8,128)S(1)}, f32[1408,512]{1,0:T(8,128)}, u32[]{:S(2)}) copy-start(f32[1408,512]{1,0:T(8,128)} %param.14) | copy-start | bytes 8650756
  103.8 29.8 %copy-start.2 = (bf16[704,512]{1,0:T(8,128)(2,1)S(1)}, bf16[704,512]{1,0:T(8,128)(2,1)}, u32[]{:S(2)}) copy-start(bf16[704,512]{1,0:T(8,128)(2,1)} %copy-done.1) | copy-start | bytes 2162692
  219.1 0.7 copy-start.4
Sparse Core Ops, SparseCore 0:
  9.7 95.3 all-gather.6
  107.0 34.7 all-gather.4
  143.3 63.4 all-gather.8
  219.3 49.8 reduce-scatter.1
